TPU v7x, 512 devices: a whole 4x4x16 slice. The times are simulated.
512 devices in a mesh: tp: 16 (over y, x), dp: 32 (over z, core).
Axes of the slice: x: 4, y: 4, z: 16, core: 2. Of those that a mesh axis runs over, the one named last changes fastest.
Arguments:
- tokens: bfloat16 [64, 4096], P('tp', 'dp'), may hold values from -12.5 to 12.5
- gain_first: bfloat16 [4096], P('dp'), may hold values from 0.099609375 to 1.8984375
- query_first: bfloat16 [4096, 2048], P('dp', 'tp'), may hold values from -0.09375 to 0.09375
- key_first: bfloat16 [4096, 2048], P('dp', 'tp'), may hold values from -0.09375 to 0.09375
- value_first: bfloat16 [4096, 4096], P('dp', 'tp'), may hold values from -0.09375 to 0.09375
- outgate_first: bfloat16 [4096, 4096], P('dp', 'tp'), may hold values from -0.09375 to 0.09375
- inputgate_first: bfloat16 [4096, 16], P('dp'), may hold values from -0.09375 to 0.09375
- forget_first: bfloat16 [4096, 16], P('dp'), may hold values from -0.09375 to 0.09375
- mixing_first: bfloat16 [4096, 4096], P('tp', 'dp'), may hold values from -0.09375 to 0.09375
- cell_first: float32 [64, 16, 256, 128], P('dp', 'tp'), may hold values from -6 to 6
- norm_first: float32 [64, 16, 128], P('dp', 'tp'), may hold values from -6 to 6
- stabilizer_first: float32 [64, 16], P('dp', 'tp'), may hold values from -3 to 115
- gain_second: bfloat16 [4096], P('dp'), may hold values from 0.099609375 to 1.8984375
- query_second: bfloat16 [4096, 2048], P('dp', 'tp'), may hold values from -0.09375 to 0.09375
- key_second: bfloat16 [4096, 2048], P('dp', 'tp'), may hold values from -0.09375 to 0.09375
- value_second: bfloat16 [4096, 4096], P('dp', 'tp'), may hold values from -0.09375 to 0.09375
- outgate_second: bfloat16 [4096, 4096], P('dp', 'tp'), may hold values from -0.09375 to 0.09375
- inputgate_second: bfloat16 [4096, 16], P('dp'), may hold values from -0.09375 to 0.09375
- forget_second: bfloat16 [4096, 16], P('dp'), may hold values from -0.09375 to 0.09375
- mixing_second: bfloat16 [4096, 4096], P('tp', 'dp'), may hold values from -0.09375 to 0.09375
- cell_second: float32 [64, 16, 256, 128], P('dp', 'tp'), may hold values from -6 to 6
- norm_second: float32 [64, 16, 128], P('dp', 'tp'), may hold values from -6 to 6
- stabilizer_second: float32 [64, 16], P('dp', 'tp'), may hold values from -3 to 115
Outputs:
- hidden: bfloat16 [64, 4096], P('tp', 'dp')
- cell_first_next: float32 [64, 16, 256, 128], P('dp', 'tp')
- norm_first_next: float32 [64, 16, 128], P('dp', 'tp')
- stabilizer_first_next: float32 [64, 16], P('dp', 'tp')
- cell_second_next: float32 [64, 16, 256, 128], P('dp', 'tp')
- norm_second_next: float32 [64, 16, 128], P('dp', 'tp')
- stabilizer_second_next: float32 [64, 16], P('dp', 'tp')
All inputs are finite; a program needn't handle non-finite values.
Results may differ from a plain program's by a relative error of at most 0.023.
Values may be sent and summed in bfloat16 or wider, within the bound.
A program may use at most 64 MiB of HBM per device.

v0:
```python
import jax
import jax.numpy as jnp
from jax import lax
from jax.sharding import PartitionSpec as P

D = 4096
DHK = 128
DHV = 256


eps = 1e-06


def copy_for_each(value, axis):
    copies = jnp.broadcast_to(value, (lax.axis_size(axis), *value.shape))
    return lax.all_to_all(copies, axis, split_axis=0, concat_axis=0, tiled=True)


def laid_out(tiles, dim):
    lengths = list(tiles.shape[1:])
    lengths[dim] *= tiles.shape[0]
    return jnp.moveaxis(tiles, 0, dim).reshape(lengths)


def gathered_copies(value, axis, dim):
    tiles = copy_for_each(value, axis)
    return laid_out(tiles, dim)


def split_up(value, dim, length):
    lengths = value.shape
    tiles = value.reshape(*lengths[:dim], length, lengths[dim] // length, *lengths[dim + 1 :])
    return jnp.moveaxis(tiles, dim, 0)


def sum_at_owner(value, axis, dim):
    tiles = split_up(value, dim, lax.axis_size(axis))
    arrived = lax.all_to_all(tiles, axis, split_axis=0, concat_axis=0, tiled=True)
    return arrived.sum(axis=0)


def side_by_side(arrays, axis, dim, along):
    columns = [a.reshape(*a.shape[:along], -1) for a in arrays]
    both = jnp.concatenate(columns, axis=along)
    filled, at, gathered = (sum_at_owner(both, axis, dim), 0, [])
    for a, column in zip(arrays, columns):
        share = filled[..., at : at + column.shape[along]]
        gathered.append(share.reshape(*share.shape[:along], *a.shape[along:]))
        at += column.shape[along]
    return tuple(gathered)


def sent_and_summed(value, axis, dim):
    length = lax.axis_size(axis)
    tiles = lax.all_to_all(split_up(value, dim, length), axis, 0, 0, tiled=True)
    return jnp.sum(tiles.astype(jnp.float32), axis=0)


def cell_step(
    x_shard,
    gain,
    w_query,
    w_key,
    w_value,
    w_outgate,
    w_input,
    w_forget,
    w_mixing,
    cell_state,
    norm_state,
    stabilizer,
):
    seq_count = cell_state.shape[0]
    local_heads = cell_state.shape[1]
    gathered = gathered_copies(x_shard, "tp", 0)
    widened = gathered.astype(jnp.float32)
    squares = jnp.sum(widened * widened, axis=1)
    scaled = (widened * gain.astype(jnp.float32)).astype(jnp.bfloat16)

    def project(weight):
        return jnp.dot(scaled, weight, preferred_element_type=jnp.float32)

    query_part, key_part, input_part, forget_part, value_part, outgate_part, own_squares = (
        side_by_side(
            (
                project(w_query),
                project(w_key),
                project(w_input),
                project(w_forget),
                project(w_value),
                project(w_outgate),
                squares,
            ),
            "dp",
            0,
            1,
        )
    )
    row_scale = lax.rsqrt(own_squares / D + eps)[:, None]
    offset = lax.axis_index("tp") * local_heads
    input_pre = lax.dynamic_slice_in_dim(input_part * row_scale, offset, local_heads, 1)
    forget_pre = lax.dynamic_slice_in_dim(forget_part * row_scale, offset, local_heads, 1)
    queries = (query_part * row_scale).reshape(seq_count, local_heads, DHK) * DHK ** (-0.5)
    key_rows = (key_part * row_scale).reshape(seq_count, local_heads, DHK)
    log_forget = jax.nn.log_sigmoid(forget_pre)
    stab_next = jnp.maximum(log_forget + stabilizer, input_pre)
    retain = jnp.exp(log_forget + stabilizer - stab_next)
    admitted = jnp.exp(input_pre - stab_next)
    kept_cell = retain[:, :, None, None] * cell_state
    kept_norm = retain[:, :, None] * norm_state
    value_rows = (value_part * row_scale).reshape(seq_count, local_heads, DHV)
    cell_next = (
        kept_cell + admitted[:, :, None, None] * value_rows[:, :, :, None] * key_rows[:, :, None, :]
    )
    norm_next = kept_norm + admitted[:, :, None] * key_rows
    numerator = jnp.einsum("shvd,shd->shv", cell_next, queries, precision=lax.Precision.HIGHEST)
    denominator = jnp.einsum("shd,shd->sh", norm_next, queries, precision=lax.Precision.HIGHEST)
    readout = numerator / jnp.maximum(jnp.abs(denominator), 1.0)[:, :, None]
    gated_rows = (
        readout.reshape(seq_count, local_heads * DHV) * jax.nn.sigmoid(outgate_part * row_scale)
    ).astype(jnp.bfloat16)
    partial_value = jnp.dot(
        gathered_copies(gated_rows, "dp", 0), w_mixing, preferred_element_type=jnp.float32
    )
    summed = sent_and_summed(partial_value.astype(jnp.bfloat16), "tp", 0)
    result = (x_shard.astype(jnp.float32) + summed).astype(jnp.bfloat16)
    return (result, cell_next, norm_next, stab_next)


def per_device(
    tokens,
    gain_first,
    query_first,
    key_first,
    value_first,
    outgate_first,
    inputgate_first,
    forget_first,
    mixing_first,
    cell_first,
    norm_first,
    stabilizer_first,
    gain_second,
    query_second,
    key_second,
    value_second,
    outgate_second,
    inputgate_second,
    forget_second,
    mixing_second,
    cell_second,
    norm_second,
    stabilizer_second,
):
    middle, cell_one, norm_one, stab_one = cell_step(
        tokens,
        gain_first,
        query_first,
        key_first,
        value_first,
        outgate_first,
        inputgate_first,
        forget_first,
        mixing_first,
        cell_first,
        norm_first,
        stabilizer_first,
    )
    hidden, cell_two, norm_two, stab_two = cell_step(
        middle,
        gain_second,
        query_second,
        key_second,
        value_second,
        outgate_second,
        inputgate_second,
        forget_second,
        mixing_second,
        cell_second,
        norm_second,
        stabilizer_second,
    )
    return (hidden, cell_one, norm_one, stab_one, cell_two, norm_two, stab_two)


def solution(mesh):
    return jax.shard_map(
        per_device,
        mesh=mesh,
        in_specs=(
            P("tp", "dp"),
            P("dp"),
            P("dp", "tp"),
            P("dp", "tp"),
            P("dp", "tp"),
            P("dp", "tp"),
            P("dp", None),
            P("dp", None),
            P("tp", "dp"),
            P("dp", "tp", None, None),
            P("dp", "tp", None),
            P("dp", "tp"),
            P("dp"),
            P("dp", "tp"),
            P("dp", "tp"),
            P("dp", "tp"),
            P("dp", "tp"),
            P("dp", None),
            P("dp", None),
            P("tp", "dp"),
            P("dp", "tp", None, None),
            P("dp", "tp", None),
            P("dp", "tp"),
        ),
        out_specs=(
            P("tp", "dp"),
            P("dp", "tp", None, None),
            P("dp", "tp", None),
            P("dp", "tp"),
            P("dp", "tp", None, None),
            P("dp", "tp", None),
            P("dp", "tp"),
        ),
        check_vma=False,
    )
```

profile of v0, /device:TPU:1, one launch (start us, length us, event | category | flops | bytes accessed | tf_op | source)
XLA Modules:
  0.0 162.5 jit_solution(5534073119439327052)
XLA Ops:
  0.6 1.3 broadcast_in_dim.8
  2.0 7.7 %all-to-all-start = ((bf16[16,4,128]{2,1,0:T(4,128)(2,1)}), bf16[16,4,128]{2,1,0:T(4,128)(2,1)S(1)}, u32[]{:S(2)}, u32[]{:S(2)}) async-start(bf16[16,4,128]{2,1,0:T(4,128)(2,1)} %broadcast_in_dim.8), calls=%async_computation | async-start | bytes 32768 | tf_op jit(solution)/shard_map/all_to_all | solution.py:16
  9.7 6.4 %all-to-all-done = bf16[16,4,128]{2,1,0:T(4,128)(2,1)S(1)} async-done(((bf16[16,4,128]{2,1,0:T(4,128)(2,1)}), bf16[16,4,128]{2,1,0:T(4,128)(2,1)S(1)}, u32[]{:S(2)}, u32[]{:S(2)}) %all-to-all-start) | async-done | bytes 16416 | tf_op jit(solution)/shard_map/all_to_all | solution.py:16
  16.3 0.7 copy-done.7
  20.7 0.9 copy.142
  21.5 17.5 %all-to-all-start.1 = ((f32[32,2,801]{2,1,0:T(2,128)}), f32[32,2,801]{2,1,0:T(2,128)S(1)}, u32[]{:S(2)}, u32[]{:S(2)}) async-start(f32[32,2,801]{2,1,0:T(2,128)} %copy.142), calls=%async_computation.1 | async-start | bytes 458752 | tf_op jit(solution)/shard_map/all_to_all | solution.py:38
  39.8 19.5 %all-to-all-done.1 = f32[32,2,801]{2,1,0:T(2,128)S(1)} async-done(((f32[32,2,801]{2,1,0:T(2,128)}), f32[32,2,801]{2,1,0:T(2,128)S(1)}, u32[]{:S(2)}, u32[]{:S(2)}) %all-to-all-start.1) | async-done | bytes 205088 | tf_op jit(solution)/shard_map/all_to_all | solution.py:38
  60.0 0.7 copy-done.19
  60.7 0.7 fusion.51
  62.1 16.3 %all_to_all.40 = bf16[32,2,256]{2,1,0:T(2,128)(2,1)S(1)} all-to-all(bf16[32,2,256]{2,1,0:T(2,128)(2,1)S(1)} %broadcast_in_dim.9), channel_id=1, replica_groups=mesh['tp'=16,'dp'=32] {'dp'}, dimensions={0} | all-to-all | bytes 65536 | tf_op jit(solution)/shard_map/all_to_all | solution.py:16
  78.6 9.2 %all_to_all.41 = bf16[16,4,128]{2,1,0:T(4,128)(2,1)S(1)} all-to-all(bf16[16,4,128]{2,1,0:T(4,128)(2,1)S(1)} %bitcast.100), channel_id=1, replica_groups=mesh['tp'=16,'dp'=32] {'tp'}, dimensions={0} | all-to-all | bytes 32768 | tf_op jit(solution)/shard_map/all_to_all | solution.py:55
  87.8 0.6 copy-done.14
  89.1 3.6 %all-to-all-start.4 = ((bf16[16,4,128]{2,1,0:T(4,128)(2,1)}), bf16[16,4,128]{2,1,0:T(4,128)(2,1)S(1)}, u32[]{:S(2)}, u32[]{:S(2)}) async-start(bf16[16,4,128]{2,1,0:T(4,128)(2,1)} %broadcast_in_dim.10), calls=%async_computation.4 | async-start | bytes 32768 | tf_op jit(solution)/shard_map/all_to_all | solution.py:16
  92.7 6.4 %all-to-all-done.4 = bf16[16,4,128]{2,1,0:T(4,128)(2,1)S(1)} async-done(((bf16[16,4,128]{2,1,0:T(4,128)(2,1)}), bf16[16,4,128]{2,1,0:T(4,128)(2,1)S(1)}, u32[]{:S(2)}, u32[]{:S(2)}) %all-to-all-start.4) | async-done | bytes 16416 | tf_op jit(solution)/shard_map/all_to_all | solution.py:16
  99.3 0.7 copy-done.9
  103.6 0.9 copy.150
  104.5 7.2 %all-to-all-start.5 = ((f32[32,2,801]{2,1,0:T(2,128)}), f32[32,2,801]{2,1,0:T(2,128)S(1)}, u32[]{:S(2)}, u32[]{:S(2)}) async-start(f32[32,2,801]{2,1,0:T(2,128)} %copy.150), calls=%async_computation.5 | async-start | bytes 458752 | tf_op jit(solution)/shard_map/all_to_all | solution.py:38
  111.8 20.2 %all-to-all-done.5 = f32[32,2,801]{2,1,0:T(2,128)S(1)} async-done(((f32[32,2,801]{2,1,0:T(2,128)}), f32[32,2,801]{2,1,0:T(2,128)S(1)}, u32[]{:S(2)}, u32[]{:S(2)}) %all-to-all-start.5) | async-done | bytes 205088 | tf_op jit(solution)/shard_map/all_to_all | solution.py:38
  132.7 0.7 copy-done.20
  133.4 0.7 fusion.50
  134.8 16.4 %all_to_all.42 = bf16[32,2,256]{2,1,0:T(2,128)(2,1)S(1)} all-to-all(bf16[32,2,256]{2,1,0:T(2,128)(2,1)S(1)} %broadcast_in_dim.11), channel_id=1, replica_groups=mesh['tp'=16,'dp'=32] {'dp'}, dimensions={0} | all-to-all | bytes 65536 | tf_op jit(solution)/shard_map/all_to_all | solution.py:16
  151.3 0.7 convolution_convert_fusion
  152.0 3.5 %all-to-all-start.7 = ((bf16[16,4,128]{2,1,0:T(4,128)(2,1)}), bf16[16,4,128]{2,1,0:T(4,128)(2,1)S(1)}, u32[]{:S(2)}, u32[]{:S(2)}) async-start(bf16[16,4,128]{2,1,0:T(4,128)(2,1)} %bitcast.29), calls=%async_computation.7 | async-start | bytes 32768 | tf_op jit(solution)/shard_map/all_to_all | solution.py:55
  156.7 5.2 %all-to-all-done.7 = bf16[16,4,128]{2,1,0:T(4,128)(2,1)S(1)} async-done(((bf16[16,4,128]{2,1,0:T(4,128)(2,1)}), bf16[16,4,128]{2,1,0:T(4,128)(2,1)S(1)}, u32[]{:S(2)}, u32[]{:S(2)}) %all-to-all-start.7) | async-done | bytes 16416 | tf_op jit(solution)/shard_map/all_to_all | solution.py:55
  (103 shorter events, 13.6 us)
Async XLA Ops:
  0.6 15.5 %copy-start = (bf16[128,256]{1,0:T(8,128)(2,1)S(1)}, bf16[128,256]{1,0:T(8,128)(2,1)}, u32[]{:S(2)}) copy-start(bf16[128,256]{1,0:T(8,128)(2,1)} %param.27) | copy-start | bytes 196612
  2.0 7.7 %copy-start.21 = (bf16[128]{0:T(256)(128)(2,1)S(1)}, bf16[128]{0:T(256)(128)(2,1)}, u32[]{:S(2)}) copy-start(bf16[128]{0:T(256)(128)(2,1)} %param.24) | copy-start | bytes 772
  2.0 14.2 %all-to-all-start = ((bf16[16,4,128]{2,1,0:T(4,128)(2,1)}), bf16[16,4,128]{2,1,0:T(4,128)(2,1)S(1)}, u32[]{:S(2)}, u32[]{:S(2)}) async-start(bf16[16,4,128]{2,1,0:T(4,128)(2,1)} %broadcast_in_dim.8), calls=%async_computation | async-start | bytes 32768 | tf_op jit(solution)/shard_map/all_to_all | solution.py:16
  16.2 0.8 copy-start.7
  17.0 0.8 copy-start.10
  17.8 0.8 copy-start.11
  21.5 39.9 %copy-start.3 = (f32[2,1,256,128]{3,2,1,0:T(8,128)S(1)}, f32[2,1,256,128]{3,2,1,0:T(8,128)}, u32[]{:S(2)}) copy-start(f32[2,1,256,128]{3,2,1,0:T(8,128)} %param.32) | copy-start | bytes 786436
  21.5 37.8 %all-to-all-start.1 = ((f32[32,2,801]{2,1,0:T(2,128)}), f32[32,2,801]{2,1,0:T(2,128)S(1)}, u32[]{:S(2)}, u32[]{:S(2)}) async-start(f32[32,2,801]{2,1,0:T(2,128)} %copy.142), calls=%async_computation.1 | async-start | bytes 458752 | tf_op jit(solution)/shard_map/all_to_all | solution.py:38
  60.0 0.7 copy-start.19
  61.6 17.0 %copy-start.1 = (f32[2,1,256,128]{3,2,1,0:T(8,128)}, f32[2,1,256,128]{3,2,1,0:T(8,128)S(1)}, u32[]{:S(2)}) copy-start(f32[2,1,256,128]{3,2,1,0:T(8,128)S(1)} %multiply_add_fusion.1) | copy-start | bytes 786436
  62.1 16.4 %copy-start.5 = (bf16[256,128]{1,0:T(8,128)(2,1)S(1)}, bf16[256,128]{1,0:T(8,128)(2,1)}, u32[]{:S(2)}) copy-start(bf16[256,128]{1,0:T(8,128)(2,1)} %param.31) | copy-start | bytes 196612
  87.8 4.9 %copy-start.23 = (bf16[128]{0:T(256)(128)(2,1)S(1)}, bf16[128]{0:T(256)(128)(2,1)}, u32[]{:S(2)}) copy-start(bf16[128]{0:T(256)(128)(2,1)} %param.35) | copy-start | bytes 772
  89.1 10.0 %copy-start.8 = (bf16[128,256]{1,0:T(8,128)(2,1)S(1)}, bf16[128,256]{1,0:T(8,128)(2,1)}, u32[]{:S(2)}) copy-start(bf16[128,256]{1,0:T(8,128)(2,1)} %param.39) | copy-start | bytes 196612
  89.1 10.0 %all-to-all-start.4 = ((bf16[16,4,128]{2,1,0:T(4,128)(2,1)}), bf16[16,4,128]{2,1,0:T(4,128)(2,1)S(1)}, u32[]{:S(2)}, u32[]{:S(2)}) async-start(bf16[16,4,128]{2,1,0:T(4,128)(2,1)} %broadcast_in_dim.10), calls=%async_computation.4 | async-start | bytes 32768 | tf_op jit(solution)/shard_map/all_to_all | solution.py:16
  99.1 0.8 copy-start.9
  100.0 0.8 copy-start.12
  100.7 0.8 copy-start.13
  104.5 7.3 %copy-start.24 = (f32[2,1]{0,1:T(1,128)S(1)}, f32[2,1]{0,1:T(1,128)}, u32[]{:S(2)}) copy-start(f32[2,1]{0,1:T(1,128)} %param.45) | copy-start | bytes 28
  104.5 29.7 %copy-start.4 = (f32[2,1,256,128]{3,2,1,0:T(8,128)S(1)}, f32[2,1,256,128]{3,2,1,0:T(8,128)}, u32[]{:S(2)}) copy-start(f32[2,1,256,128]{3,2,1,0:T(8,128)} %param.43) | copy-start | bytes 786436
  104.5 27.6 %all-to-all-start.5 = ((f32[32,2,801]{2,1,0:T(2,128)}), f32[32,2,801]{2,1,0:T(2,128)S(1)}, u32[]{:S(2)}, u32[]{:S(2)}) async-start(f32[32,2,801]{2,1,0:T(2,128)} %copy.150), calls=%async_computation.5 | async-start | bytes 458752 | tf_op jit(solution)/shard_map/all_to_all | solution.py:38
  132.7 0.7 copy-start.20
  134.3 17.7 %copy-start.2 = (f32[2,1,256,128]{3,2,1,0:T(8,128)}, f32[2,1,256,128]{3,2,1,0:T(8,128)S(1)}, u32[]{:S(2)}) copy-start(f32[2,1,256,128]{3,2,1,0:T(8,128)S(1)} %multiply_add_fusion) | copy-start | bytes 786436
  134.8 16.5 %copy-start.6 = (bf16[256,128]{1,0:T(8,128)(2,1)S(1)}, bf16[256,128]{1,0:T(8,128)(2,1)}, u32[]{:S(2)}) copy-start(bf16[256,128]{1,0:T(8,128)(2,1)} %param.42) | copy-start | bytes 196612
  152.0 9.9 %all-to-all-start.7 = ((bf16[16,4,128]{2,1,0:T(4,128)(2,1)}), bf16[16,4,128]{2,1,0:T(4,128)(2,1)S(1)}, u32[]{:S(2)}, u32[]{:S(2)}) async-start(bf16[16,4,128]{2,1,0:T(4,128)(2,1)} %bitcast.29), calls=%async_computation.7 | async-start | bytes 32768 | tf_op jit(solution)/shard_map/all_to_all | solution.py:55
  (6 other events, 4.1 us)
where the time goes:
time: 164 us; the launch traced here: 162 us
  waiting for transfers between devices  57.7 us (35%)
  blocking collectives  42 us (26%)
  starting transfers between devices  39.6 us (24%)
  local copies, waits for them, and re-layouts  15.1 us (9%)
  other arithmetic  4.19 us (3%)
  matrix products  3.01 us (2%)
    all_to_all x2, waiting for transfers between devices, sum_at_owner(): lax.all_to_all(tiles, axis, split_axis=0, concat_axis=0, tiled=True)  39.7 us
    all_to_all x2, blocking collectives, copy_for_each(): return lax.all_to_all(copies, axis, split_axis=0, concat_axis=0, tiled=True)  32.8 us
    all_to_all x2, starting transfers between devices, sum_at_owner(): lax.all_to_all(tiles, axis, split_axis=0, concat_axis=0, tiled=True)  24.7 us
    all_to_all x2, waiting for transfers between devices, copy_for_each(): return lax.all_to_all(copies, axis, split_axis=0, concat_axis=0, tiled=True)  12.8 us
    all_to_all x2, starting transfers between devices, copy_for_each(): return lax.all_to_all(copies, axis, split_axis=0, concat_axis=0, tiled=True)  11.3 us
    unnamed x54, local copies, waits for them, and re-layouts  10.3 us
    all_to_all x1, blocking collectives, sent_and_summed(): tiles = lax.all_to_all(split_up(value, dim, length), axis, 0, 0, tiled=True)  9.18 us
    all_to_all x1, waiting for transfers between devices, sent_and_summed(): tiles = lax.all_to_all(split_up(value, dim, length), axis, 0, 0, tiled=True)  5.18 us
  transfers between devices with their start and end apart: 5, of which 5 were waited for; matrix products, arithmetic and copies ran while one was open for 1% of the time, Pallas kernels for 0%

commit v1 on v0

v1 whole, which is shorter than its diff:
```python
import functools

import jax
import jax.numpy as jnp
from jax import lax
from jax.experimental import pallas as pl
from jax.experimental.pallas import tpu as pltpu
from jax.sharding import PartitionSpec as P

DHK = 128
DHV = 256
EPS = 1e-06
ROWS = 16
MESH = pl.DeviceIdType.MESH
F32 = jnp.float32
BF16 = jnp.bfloat16


def kernel(T, N, *refs):
    (x_in, *rest) = refs
    ins = (rest[:11], rest[11:22])
    outs = rest[22:29]
    (
        wcat,
        wmix,
        wif,
        wif_own,
        gains,
        cell,
        norm,
        stab,
        cellt_hi,
        cellt_lo,
        xg,
        xs,
        stage,
        sbuf,
        rbuf,
        gbuf,
        gs,
        ybuf,
        ysc,
        ysend,
        yrecv,
        load_sems,
        out_sems,
        send_sems,
        recv_sems,
    ) = rest[29:]
    t = lax.axis_index("tp")
    d = lax.axis_index("dp")
    features = DHK * N

    def tp_peer(o):
        return {"tp": lax.rem(t + o, T)}

    def dp_peer(o):
        return {"dp": lax.rem(d + o, N)}

    far_dp = sorted(range(1, N), key=lambda o: abs(o - N // 2))

    x_load = pltpu.make_async_copy(x_in, xg.at[t], load_sems.at[0])
    x_load.start()
    loads = []
    for c in range(2):
        gain, wq, wk, wv, wo, wi, wf, wm, state, nstate, mstate = ins[c]
        pairs = [
            (gain, gains.at[c]),
            (wq, wcat.at[c, :, 0:128]),
            (wk, wcat.at[c, :, 128:256]),
            (wv, wcat.at[c, :, 256:512]),
            (wo, wcat.at[c, :, 512:768]),
            (wi, wif.at[c, 0]),
            (wf, wif.at[c, 1]),
            (state, cell.at[c]),
            (nstate, norm.at[c]),
            (mstate, stab.at[c]),
            (wm, wmix.at[c]),
        ]
        group = []
        for n, (src, dst) in enumerate(pairs):
            copy = pltpu.make_async_copy(src, dst, load_sems.at[1 + 11 * c + n])
            copy.start()
            group.append(copy)
        loads.append(group)

    barrier = pltpu.get_barrier_semaphore()
    for o in far_dp:
        pl.semaphore_signal(barrier, inc=1, device_id=dp_peer(o), device_id_type=MESH)
    for o in range(1, T):
        pl.semaphore_signal(barrier, inc=1, device_id=tp_peer(o), device_id_type=MESH)

    def prepare(c):
        mine = lax.broadcasted_iota(jnp.int32, (T, DHK), 0) == t
        for g in range(2):
            wif_own[c, g] = jnp.sum(jnp.where(mine, wif[c, g].astype(F32), 0.0), axis=0, keepdims=True)
        for s in range(2):
            old = cell[c, s * DHV : (s + 1) * DHV, :]
            turned = old.T
            high = turned.astype(BF16)
            cellt_hi[c, :, s * DHV : (s + 1) * DHV] = high
            cellt_lo[c, :, s * DHV : (s + 1) * DHV] = (turned - high.astype(F32)).astype(BF16)

    for copy in loads[0]:
        copy.wait()
    prepare(0)

    pl.semaphore_wait(barrier, T + N - 2)

    x_load.wait()
    sends = []

    def send(src, dst, phase, peer):
        copy = pltpu.make_async_remote_copy(
            src_ref=src,
            dst_ref=dst,
            send_sem=send_sems.at[phase],
            recv_sem=recv_sems.at[phase],
            device_id=peer,
            device_id_type=MESH,
        )
        copy.start()
        return copy

    def wait_recv(ref, phase):
        pltpu.make_async_copy(ref, ref, recv_sems.at[phase]).wait()

    def wait_send(ref, phase):
        pltpu.make_async_copy(ref, ref, send_sems.at[phase]).wait()

    for o in range(1, T):
        send(xg.at[t], xg.at[t], 0, tp_peer(o))
    sends.append((xg.at[pl.ds(0, T - 1)], 0))

    for copy in loads[1]:
        copy.wait()
    prepare(1)

    wait_recv(xg.at[pl.ds(0, T - 1)], 0)
    for j in range(T):
        xs[4 * j : 4 * j + 4, :] = xg[j].astype(F32)

    def project(c, phase):
        wide = jnp.concatenate([xs[pl.ds(0, N, stride=2), :], xs[pl.ds(1, N, stride=2), :]], axis=0)
        scaled = (wide * gains[c].astype(F32)).astype(BF16)
        squares = jnp.sum(wide * wide, axis=1, keepdims=True)
        scaled_wide = scaled.astype(F32)
        wi_row = wif_own[c, 0]
        wf_row = wif_own[c, 1]
        i_part = jnp.sum(scaled_wide * wi_row, axis=1, keepdims=True)
        f_part = jnp.sum(scaled_wide * wf_row, axis=1, keepdims=True)
        lane = lax.broadcasted_iota(jnp.int32, (2 * N, 128), 1)
        misc = jnp.where(lane == 0, i_part, jnp.where(lane == 1, f_part, squares))
        high = misc.astype(BF16).astype(F32)
        low = misc - high
        product = jnp.dot(scaled, wcat[c], preferred_element_type=F32)
        blocks = [product[:, 128 * b : 128 * (b + 1)] for b in range(6)] + [high, low]
        for b, block in enumerate(blocks):
            for s in range(2):
                stage[pl.ds(2 * b + s, N, stride=ROWS), :] = block[s * N : (s + 1) * N]
        sbuf[c] = stage[...].reshape(N, ROWS, 128).astype(BF16)
        for o in far_dp:
            send(sbuf.at[c, lax.rem(d + o, N)], rbuf.at[c, N - 1 - o], phase, dp_peer(o))
        sends.append((rbuf.at[c], phase))

    def step_state(c, phase_in, phase_out):
        wait_recv(rbuf.at[c], phase_in)
        acc = sbuf[c, d].astype(F32) + jnp.sum(rbuf[c].astype(F32), axis=0)
        acc_hi = acc.astype(BF16)
        acc_lo = (acc - acc_hi.astype(F32)).astype(BF16)
        read = (
            jnp.dot(acc_hi, cellt_hi[c], preferred_element_type=F32)
            + jnp.dot(acc_lo, cellt_hi[c], preferred_element_type=F32)
            + jnp.dot(acc_hi, cellt_lo[c], preferred_element_type=F32)
        )
        row = lax.broadcasted_iota(jnp.int32, (2, DHV), 0)
        read = jnp.where(row == 0, read[0:2, 0:DHV], read[0:2, DHV : 2 * DHV])
        q0 = acc[0:2]
        k0 = acc[2:4]
        v0 = jnp.concatenate([acc[4:6], acc[6:8]], axis=1)
        o0 = jnp.concatenate([acc[8:10], acc[10:12]], axis=1)
        misc = acc[12:14] + acc[14:16]
        lane = lax.broadcasted_iota(jnp.int32, (2, 128), 1)
        i0 = jnp.sum(jnp.where(lane == 0, misc, 0.0), axis=1, keepdims=True)
        f0 = jnp.sum(jnp.where(lane == 1, misc, 0.0), axis=1, keepdims=True)
        squares = jnp.sum(jnp.where(lane == 2, misc, 0.0), axis=1, keepdims=True)
        kq0 = jnp.sum(k0 * q0, axis=1, keepdims=True)
        nq0 = jnp.sum(norm[c] * q0, axis=1, keepdims=True)
        r = lax.rsqrt(squares / features + EPS)
        rq = r * DHK ** (-0.5)
        i_pre = i0 * r
        f_pre = f0 * r
        pick = lax.broadcasted_iota(jnp.int32, (2, 2), 0) == lax.broadcasted_iota(jnp.int32, (2, 2), 1)
        m = jnp.sum(jnp.where(pick, stab[c], 0.0), axis=1, keepdims=True)
        lf = jnp.minimum(f_pre, 0.0) - jnp.log1p(jnp.exp(-jnp.abs(f_pre)))
        m_next = jnp.maximum(lf + m, i_pre)
        retain = jnp.exp(lf + m - m_next)
        admit = jnp.exp(i_pre - m_next)
        kq = kq0 * r * rq
        den = retain * (nq0 * rq) + admit * kq
        num = (retain * rq) * read + (admit * kq) * (v0 * r)
        gated = num / jnp.maximum(jnp.abs(den), 1.0) * jax.nn.sigmoid(o0 * r)
        gbuf[c, d] = gated.astype(BF16)
        for o in far_dp:
            send(gbuf.at[c, d], gbuf.at[c, d], phase_out, dp_peer(o))
        sends.append((gbuf.at[c, pl.ds(0, N - 1)], phase_out))
        _, c_out, n_out, m_out = None, *outs[1 + 3 * c : 4 + 3 * c]
        k = k0 * r
        n_out[...] = retain * norm[c] + admit * k
        m_out[...] = jnp.sum(jnp.where(pick, m_next, 0.0), axis=0, keepdims=True)
        va = v0 * (r * admit)
        for s in range(2):
            column = jnp.broadcast_to(va[s : s + 1], (8, DHV)).T[:, 0:1]
            cell[c, s * DHV : (s + 1) * DHV, :] = (
                retain[s : s + 1] * cell[c, s * DHV : (s + 1) * DHV, :] + column * k[s : s + 1]
            )
        copy = pltpu.make_async_copy(cell.at[c], c_out, out_sems.at[c])
        copy.start()
        return copy

    def mix(c, phase_in):
        wait_recv(gbuf.at[c, pl.ds(0, N - 1)], phase_in)
        for j in range(N):
            gs[2 * j : 2 * j + 2, :] = gbuf[c, j].astype(F32)
        return jnp.dot(gs[...].astype(BF16), wmix[c], preferred_element_type=F32)

    project(0, 1)
    out_first = step_state(0, 1, 2)
    partial = mix(0, 2)
    ybuf[t] = partial.astype(BF16)
    for o in range(1, T):
        send(ybuf.at[t], ybuf.at[t], 3, tp_peer(o))
    sends.append((ybuf.at[pl.ds(0, T - 1)], 3))
    wait_recv(ybuf.at[pl.ds(0, T - 1)], 3)
    middle = xs[...] + jnp.sum(ybuf[...].astype(F32), axis=0)
    xs[...] = middle.astype(BF16).astype(F32)
    project(1, 4)
    out_second = step_state(1, 4, 5)
    ysc[...] = mix(1, 5)
    for j in range(T):
        ysend[j] = ysc[4 * j : 4 * j + 4, :].astype(BF16)
    for o in range(1, T):
        send(ysend.at[lax.rem(t + o, T)], yrecv.at[T - 1 - o], 6, tp_peer(o))
    sends.append((yrecv, 6))
    own = xs[pl.ds(4 * t, 4), :] + ysc[pl.ds(4 * t, 4), :]
    wait_recv(yrecv, 6)
    outs[0][...] = (own + jnp.sum(yrecv[...].astype(F32), axis=0)).astype(BF16)
    out_first.wait()
    out_second.wait()
    for ref, phase in sends:
        wait_send(ref, phase)


def build(T, N):
    def per_device(*args):
        x = args[0]
        flat = [x]
        for c in range(2):
            gain, wq, wk, wv, wo, wi, wf, wm, state, nstate, mstate = args[1 + 11 * c : 12 + 11 * c]
            flat += [
                gain.reshape(1, DHK),
                wq,
                wk,
                wv,
                wo,
                wi.T,
                wf.T,
                wm,
                state.reshape(2 * DHV, DHK),
                nstate.reshape(2, DHK),
                mstate.T,
            ]
        hbm = pl.BlockSpec(memory_space=pl.ANY)
        vmem = pl.BlockSpec(memory_space=pltpu.VMEM)
        state_shapes = [
            jax.ShapeDtypeStruct((2 * DHV, DHK), F32),
            jax.ShapeDtypeStruct((2, DHK), F32),
            jax.ShapeDtypeStruct((1, 2), F32),
        ]
        B = 4 * T
        got = pl.pallas_call(
            functools.partial(kernel, T, N),
            out_shape=[jax.ShapeDtypeStruct((4, DHK), BF16)] + state_shapes * 2,
            in_specs=[hbm] * len(flat),
            out_specs=[vmem] + [hbm, vmem, vmem] * 2,
            scratch_shapes=[
                pltpu.VMEM((2, DHK, 768), BF16),
                pltpu.VMEM((2, DHV, DHK), BF16),
                pltpu.VMEM((2, 2, T, DHK), BF16),
                pltpu.VMEM((2, 2, 1, DHK), F32),
                pltpu.VMEM((2, 1, DHK), BF16),
                pltpu.VMEM((2, 2 * DHV, DHK), F32),
                pltpu.VMEM((2, 2, DHK), F32),
                pltpu.VMEM((2, 1, 2), F32),
                pltpu.VMEM((2, DHK, 2 * DHV), BF16),
                pltpu.VMEM((2, DHK, 2 * DHV), BF16),
                pltpu.VMEM((T, 4, DHK), BF16),
                pltpu.VMEM((B, DHK), F32),
                pltpu.VMEM((N * ROWS, DHK), F32),
                pltpu.VMEM((2, N, ROWS, DHK), BF16),
                pltpu.VMEM((2, N - 1, ROWS, DHK), BF16),
                pltpu.VMEM((2, N, 2, DHV), BF16),
                pltpu.VMEM((B, DHV), F32),
                pltpu.VMEM((T, B, DHK), BF16),
                pltpu.VMEM((B, DHK), F32),
                pltpu.VMEM((T, 4, DHK), BF16),
                pltpu.VMEM((T - 1, 4, DHK), BF16),
                pltpu.SemaphoreType.DMA((23,)),
                pltpu.SemaphoreType.DMA((2,)),
                pltpu.SemaphoreType.DMA((7,)),
                pltpu.SemaphoreType.DMA((7,)),
            ],
            compiler_params=pltpu.CompilerParams(collective_id=0, has_side_effects=True),
            name="cells",
        )(*flat)
        hidden, c1, n1, m1, c2, n2, m2 = got
        return (
            hidden,
            c1.reshape(2, 1, DHV, DHK),
            n1.reshape(2, 1, DHK),
            m1.T,
            c2.reshape(2, 1, DHV, DHK),
            n2.reshape(2, 1, DHK),
            m2.T,
        )

    return per_device


def solution(mesh):
    cell_specs = (
        P("dp"),
        P("dp", "tp"),
        P("dp", "tp"),
        P("dp", "tp"),
        P("dp", "tp"),
        P("dp", None),
        P("dp", None),
        P("tp", "dp"),
        P("dp", "tp", None, None),
        P("dp", "tp", None),
        P("dp", "tp"),
    )
    state_specs = (P("dp", "tp", None, None), P("dp", "tp", None), P("dp", "tp"))
    return jax.shard_map(
        build(mesh.shape["tp"], mesh.shape["dp"]),
        mesh=mesh,
        in_specs=(P("tp", "dp"),) + cell_specs * 2,
        out_specs=(P("tp", "dp"),) + state_specs * 2,
        check_vma=False,
    )
```

time: 164 us -> 72.6 us (0.44)
  Pallas kernels: 0 us -> 65.8 us
  waiting for transfers between devices: 57.7 us -> 0 us
  blocking collectives: 42 us -> 0 us
  starting transfers between devices: 39.6 us -> 0 us
  local copies, waits for them, and re-layouts: 15.1 us -> 5.91 us
  other arithmetic: 4.19 us -> 0 us
  matrix products: 3.01 us -> 0 us
    pallas_call x0 -> x1, Pallas kernels: none -> 65.8 us  [per_device(): pl.pallas_call(functools.partial(kernel, T, N), out_shape=[jax.ShapeDtype...]
    all_to_all x5 -> x0, waiting for transfers between devices: 57.7 us -> none  [the longest x2 39.7 us: sum_at_owner(): lax.all_to_all(tiles, axis, split_axis=0, concat_axis=0, tiled=True)]
    all_to_all x3 -> x0, blocking collectives: 42 us -> none  [the longest x2 32.8 us: copy_for_each(): return lax.all_to_all(copies, axis, split_axis=0, concat_axis=0, tiled=True)]
    all_to_all x5 -> x0, starting transfers between devices: 39.6 us -> none  [the longest x2 24.7 us: sum_at_owner(): lax.all_to_all(tiles, axis, split_axis=0, concat_axis=0, tiled=True)]
    unnamed x54 -> x19, local copies, waits for them, and re-layouts: 10.3 us -> 5.91 us
    dot_general x16 -> x0, matrix products: 3.01 us -> none  [the longest x12 1.49 us: project(): return jnp.dot(scaled, weight, preferred_element_type=jnp.float32)]
    concatenate x8 -> x0, local copies, waits for them, and re-layouts: 2.8 us -> none  [side_by_side(): both = jnp.concatenate(columns, axis=along)]
    broadcast_in_dim x4 -> x0, local copies, waits for them, and re-layouts: 1.98 us -> none  [copy_for_each(): copies = jnp.broadcast_to(value, (lax.axis_size(axis), *value.shape))]
  transfers between devices with their start and end apart: 5 -> 0, of which waited for: 5 -> 0; matrix products, arithmetic and copies ran while one was open for 1% -> 0% of each run, Pallas kernels for 0% -> 0%
where the time goes in v1:
time: 72.6 us; the launch traced here: 72.4 us
  Pallas kernels  65.8 us (91%)
  local copies, waits for them, and re-layouts  5.91 us (8%)
    pallas_call x1, Pallas kernels, per_device(): pl.pallas_call(functools.partial(kernel, T, N), out_shape=[jax.ShapeDtype...  65.8 us
    unnamed x19, local copies, waits for them, and re-layouts  5.91 us

profile of v1, /device:TPU:1, one launch (start us, length us, event | category | flops | bytes accessed | tf_op | source)
XLA Modules:
  0.0 72.4 jit_solution(3040284325198273097)
XLA Ops:
  0.6 65.8 %cells.1 = (bf16[4,128]{1,0:T(4,128)(2,1)}, f32[512,128]{1,0:T(8,128)}, f32[2,128]{1,0:T(2,128)}, f32[1,2]{1,0:T(1,128)}, f32[512,128]{1,0:T(8,128)}, /*index=5*/f32[2,128]{1,0:T(2,128)}, f32[1,2]{1,0:T(1,128)}) custom-call(bf16[4,128]{1,0:T(4,128)(2,1)} %refs_0_.1, bf16[1,128]{1,0:T(2,128)(2,1)} %bitcast.38, bf16[128,128]{1,0:T(8,128)(2,1)} %refs_2_.1, ...), custom_call_target="tpu_custom_call" | custom-call | tf_op jit(solution)/shard_map/cells/pallas_call | solution.py:281
  66.5 0.0 copy-start.3
  66.5 0.7 copy-done.3
  67.1 0.6 copy.41
  67.7 0.0 copy-start.2
  67.7 0.0 copy-start
  67.7 1.7 %copy.42 = f32[2,1,256,128]{3,2,1,0:T(8,128)} copy(f32[2,1,256,128]{3,2,1,0:T(8,128)} %bitcast.29) | data formatting | bytes 524288
  69.4 0.0 copy-done.2
  69.4 0.0 copy-start.5
  69.4 0.6 copy.43
  70.0 0.1 copy-done.5
  70.0 0.5 copy.44
  70.5 0.0 copy-done
  70.6 0.0 copy-start.1
  70.6 0.7 copy.45
  71.3 0.0 copy-done.1
  71.3 0.0 copy-start.4
  71.3 0.6 copy.46
  71.8 0.0 copy-done.4
  71.9 0.5 copy.47
Async XLA Ops:
  66.5 0.7 copy-start.3
  67.7 1.7 %copy-start.2 = (f32[2,128]{1,0:T(2,128)S(1)}, f32[2,128]{1,0:T(2,128)}, u32[]{:S(2)}) copy-start(f32[2,128]{1,0:T(2,128)} %get-tuple-element.16) | copy-start | bytes 3076
  67.7 2.9 %copy-start = (f32[512,128]{1,0:T(8,128)S(1)}, f32[512,128]{1,0:T(8,128)}, u32[]{:S(2)}) copy-start(f32[512,128]{1,0:T(8,128)} %get-tuple-element.18) | copy-start | bytes 786436
  69.4 0.6 copy-start.5
  70.6 0.7 copy-start.1
  71.3 0.6 copy-start.4

commit v2 on v1

--- a/solution.py
+++ b/solution.py
@@ -43,7 +43,6 @@
         ysend,
         yrecv,
         load_sems,
-        out_sems,
         send_sems,
         recv_sems,
     ) = rest[29:]
@@ -58,6 +57,12 @@
         return {"dp": lax.rem(d + o, N)}
 
     far_dp = sorted(range(1, N), key=lambda o: abs(o - N // 2))
+
+    barrier = pltpu.get_barrier_semaphore()
+    for o in far_dp:
+        pl.semaphore_signal(barrier, inc=1, device_id=dp_peer(o), device_id_type=MESH)
+    for o in range(1, T):
+        pl.semaphore_signal(barrier, inc=1, device_id=tp_peer(o), device_id_type=MESH)
 
     x_load = pltpu.make_async_copy(x_in, xg.at[t], load_sems.at[0])
     x_load.start()
@@ -84,12 +89,6 @@
             group.append(copy)
         loads.append(group)
 
-    barrier = pltpu.get_barrier_semaphore()
-    for o in far_dp:
-        pl.semaphore_signal(barrier, inc=1, device_id=dp_peer(o), device_id_type=MESH)
-    for o in range(1, T):
-        pl.semaphore_signal(barrier, inc=1, device_id=tp_peer(o), device_id_type=MESH)
-
     def prepare(c):
         mine = lax.broadcasted_iota(jnp.int32, (T, DHK), 0) == t
         for g in range(2):
@@ -101,11 +100,8 @@
             cellt_hi[c, :, s * DHV : (s + 1) * DHV] = high
             cellt_lo[c, :, s * DHV : (s + 1) * DHV] = (turned - high.astype(F32)).astype(BF16)
 
-    for copy in loads[0]:
-        copy.wait()
-    prepare(0)
-
-    pl.semaphore_wait(barrier, T + N - 2)
+    with jax.named_scope("entry"):
+        pl.semaphore_wait(barrier, T + N - 2)
 
     x_load.wait()
     sends = []
@@ -132,11 +128,12 @@
         send(xg.at[t], xg.at[t], 0, tp_peer(o))
     sends.append((xg.at[pl.ds(0, T - 1)], 0))
 
-    for copy in loads[1]:
+    for copy in loads[0]:
         copy.wait()
-    prepare(1)
-
-    wait_recv(xg.at[pl.ds(0, T - 1)], 0)
+    prepare(0)
+
+    with jax.named_scope("x_wait"):
+        wait_recv(xg.at[pl.ds(0, T - 1)], 0)
     for j in range(T):
         xs[4 * j : 4 * j + 4, :] = xg[j].astype(F32)
 
@@ -159,12 +156,14 @@
             for s in range(2):
                 stage[pl.ds(2 * b + s, N, stride=ROWS), :] = block[s * N : (s + 1) * N]
         sbuf[c] = stage[...].reshape(N, ROWS, 128).astype(BF16)
-        for o in far_dp:
-            send(sbuf.at[c, lax.rem(d + o, N)], rbuf.at[c, N - 1 - o], phase, dp_peer(o))
+        with jax.named_scope("rs_send"):
+            for o in far_dp:
+                send(sbuf.at[c, lax.rem(d + o, N)], rbuf.at[c, N - 1 - o], phase, dp_peer(o))
         sends.append((rbuf.at[c], phase))
 
     def step_state(c, phase_in, phase_out):
-        wait_recv(rbuf.at[c], phase_in)
+        with jax.named_scope("rs_wait"):
+            wait_recv(rbuf.at[c], phase_in)
         acc = sbuf[c, d].astype(F32) + jnp.sum(rbuf[c].astype(F32), axis=0)
         acc_hi = acc.astype(BF16)
         acc_lo = (acc - acc_hi.astype(F32)).astype(BF16)
@@ -201,41 +200,44 @@
         num = (retain * rq) * read + (admit * kq) * (v0 * r)
         gated = num / jnp.maximum(jnp.abs(den), 1.0) * jax.nn.sigmoid(o0 * r)
         gbuf[c, d] = gated.astype(BF16)
-        for o in far_dp:
-            send(gbuf.at[c, d], gbuf.at[c, d], phase_out, dp_peer(o))
+        with jax.named_scope("ag_send"):
+            for o in far_dp:
+                send(gbuf.at[c, d], gbuf.at[c, d], phase_out, dp_peer(o))
         sends.append((gbuf.at[c, pl.ds(0, N - 1)], phase_out))
-        _, c_out, n_out, m_out = None, *outs[1 + 3 * c : 4 + 3 * c]
+        c_out, n_out, m_out = outs[1 + 3 * c : 4 + 3 * c]
         k = k0 * r
         n_out[...] = retain * norm[c] + admit * k
         m_out[...] = jnp.sum(jnp.where(pick, m_next, 0.0), axis=0, keepdims=True)
         va = v0 * (r * admit)
         for s in range(2):
             column = jnp.broadcast_to(va[s : s + 1], (8, DHV)).T[:, 0:1]
-            cell[c, s * DHV : (s + 1) * DHV, :] = (
+            c_out[s * DHV : (s + 1) * DHV, :] = (
                 retain[s : s + 1] * cell[c, s * DHV : (s + 1) * DHV, :] + column * k[s : s + 1]
             )
-        copy = pltpu.make_async_copy(cell.at[c], c_out, out_sems.at[c])
-        copy.start()
-        return copy
 
     def mix(c, phase_in):
-        wait_recv(gbuf.at[c, pl.ds(0, N - 1)], phase_in)
+        with jax.named_scope("ag_wait"):
+            wait_recv(gbuf.at[c, pl.ds(0, N - 1)], phase_in)
         for j in range(N):
             gs[2 * j : 2 * j + 2, :] = gbuf[c, j].astype(F32)
         return jnp.dot(gs[...].astype(BF16), wmix[c], preferred_element_type=F32)
 
     project(0, 1)
-    out_first = step_state(0, 1, 2)
+    for copy in loads[1]:
+        copy.wait()
+    prepare(1)
+    step_state(0, 1, 2)
     partial = mix(0, 2)
     ybuf[t] = partial.astype(BF16)
     for o in range(1, T):
         send(ybuf.at[t], ybuf.at[t], 3, tp_peer(o))
     sends.append((ybuf.at[pl.ds(0, T - 1)], 3))
-    wait_recv(ybuf.at[pl.ds(0, T - 1)], 3)
+    with jax.named_scope("ar_wait"):
+        wait_recv(ybuf.at[pl.ds(0, T - 1)], 3)
     middle = xs[...] + jnp.sum(ybuf[...].astype(F32), axis=0)
     xs[...] = middle.astype(BF16).astype(F32)
     project(1, 4)
-    out_second = step_state(1, 4, 5)
+    step_state(1, 4, 5)
     ysc[...] = mix(1, 5)
     for j in range(T):
         ysend[j] = ysc[4 * j : 4 * j + 4, :].astype(BF16)
@@ -243,12 +245,20 @@
         send(ysend.at[lax.rem(t + o, T)], yrecv.at[T - 1 - o], 6, tp_peer(o))
     sends.append((yrecv, 6))
     own = xs[pl.ds(4 * t, 4), :] + ysc[pl.ds(4 * t, 4), :]
-    wait_recv(yrecv, 6)
+    with jax.named_scope("y_wait"):
+        wait_recv(yrecv, 6)
     outs[0][...] = (own + jnp.sum(yrecv[...].astype(F32), axis=0)).astype(BF16)
-    out_first.wait()
-    out_second.wait()
     for ref, phase in sends:
         wait_send(ref, phase)
+
+
+def publish(*refs):
+    sems = refs[14]
+    copies = [pltpu.make_async_copy(refs[n], refs[7 + n], sems.at[n]) for n in range(7)]
+    for copy in copies:
+        copy.start()
+    for copy in copies:
+        copy.wait()
 
 
 def build(T, N):
@@ -270,19 +280,20 @@
                 nstate.reshape(2, DHK),
                 mstate.T,
             ]
-        hbm = pl.BlockSpec(memory_space=pl.ANY)
+        hbm = pl.BlockSpec(memory_space=pltpu.HBM)
         vmem = pl.BlockSpec(memory_space=pltpu.VMEM)
         state_shapes = [
-            jax.ShapeDtypeStruct((2 * DHV, DHK), F32),
-            jax.ShapeDtypeStruct((2, DHK), F32),
-            jax.ShapeDtypeStruct((1, 2), F32),
+            ((2 * DHV, DHK), F32),
+            ((2, DHK), F32),
+            ((1, 2), F32),
         ]
+        shapes = [((4, DHK), BF16)] + state_shapes * 2
         B = 4 * T
         got = pl.pallas_call(
             functools.partial(kernel, T, N),
-            out_shape=[jax.ShapeDtypeStruct((4, DHK), BF16)] + state_shapes * 2,
+            out_shape=[pltpu.VMEM(*shape) for shape in shapes],
             in_specs=[hbm] * len(flat),
-            out_specs=[vmem] + [hbm, vmem, vmem] * 2,
+            out_specs=[vmem] * 7,
             scratch_shapes=[
                 pltpu.VMEM((2, DHK, 768), BF16),
                 pltpu.VMEM((2, DHV, DHK), BF16),
@@ -306,13 +317,23 @@
                 pltpu.VMEM((T, 4, DHK), BF16),
                 pltpu.VMEM((T - 1, 4, DHK), BF16),
                 pltpu.SemaphoreType.DMA((23,)),
-                pltpu.SemaphoreType.DMA((2,)),
                 pltpu.SemaphoreType.DMA((7,)),
                 pltpu.SemaphoreType.DMA((7,)),
             ],
-            compiler_params=pltpu.CompilerParams(collective_id=0, has_side_effects=True),
+            compiler_params=pltpu.CompilerParams(
+                collective_id=0, has_side_effects=True, vmem_limit_bytes=24 * 1024 * 1024
+            ),
             name="cells",
-        )(*flat)
+        )(*[pltpu.with_memory_space_constraint(a, pltpu.HBM) for a in flat])
+        got = pl.pallas_call(
+            publish,
+            out_shape=[jax.ShapeDtypeStruct(*shape) for shape in shapes],
+            in_specs=[vmem] * 7,
+            out_specs=[hbm] * 7,
+            scratch_shapes=[pltpu.SemaphoreType.DMA((7,))],
+            compiler_params=pltpu.CompilerParams(vmem_limit_bytes=1024 * 1024),
+            name="publish",
+        )(*got)
         hidden, c1, n1, m1, c2, n2, m2 = got
         return (
             hidden,

time: 72.6 us -> 67 us (0.923)
  local copies, waits for them, and re-layouts: 5.91 us -> 0 us
    unnamed x19 -> x0, local copies, waits for them, and re-layouts: 5.91 us -> none
    pallas_call x1 -> x2, Pallas kernels: 65.8 us -> 66.2 us  [the longest x1 65.3 us: per_device(): pl.pallas_call(functools.partial(kernel, T, N), out_shape=[pltpu.VMEM(*sh...]
where the time goes in v2:
time: 67 us; the launch traced here: 66.8 us
  Pallas kernels  66.2 us (99%)
    pallas_call x1, Pallas kernels, per_device(): pl.pallas_call(functools.partial(kernel, T, N), out_shape=[pltpu.VMEM(*sh...  65.3 us

profile of v2, /device:TPU:1, one launch (start us, length us, event | category | flops | bytes accessed | tf_op | source)
XLA Modules:
  0.0 66.8 jit_solution(9113217204307739323)
XLA Ops:
  0.6 65.3 %cells.1 = (bf16[4,128]{1,0:T(4,128)(2,1)S(1)}, f32[512,128]{1,0:T(8,128)S(1)}, f32[2,128]{1,0:T(2,128)S(1)}, f32[1,2]{1,0:T(1,128)S(1)}, f32[512,128]{1,0:T(8,1...) custom-call(bf16[4,128]{1,0:T(4,128)(2,1)} %refs_0_.1, bf16[1,128]{1,0:T(2,128)(2,1)} %bitcast.34, ...), custom_call_target="tpu_custom_call" | custom-call | tf_op jit(solution)/shard_map/cells/pallas_call | solution.py:292
  66.0 0.9 %publish.1 = (bf16[4,128]{1,0:T(4,128)(2,1)}, f32[512,128]{1,0:T(8,128)}, f32[2,128]{1,0:T(2,128)}, f32[1,2]{1,0:T(1,128)}, f32[512,128]{1,0:T(8,128)}, /*index=5*/f32[2,128]{1,0:T(2,128)}, f32[1,2]{1,0:T(1,128)}) custom-call(bf16[4,128]{1,0:T(4,128)(2,1)S(1)} %get-tuple-element.21.refs_0_, f32[512,128]{1,0:T(8,128)S(1)} %get-tuple-element.22.refs_1_, ...), custom_call_target="tpu_custom_call" | custom-call | tf_op jit(solution)/shard_map/publish/pallas_call | solution.py:328

commit v3 on v2

v3 whole, which is shorter than its diff:
```python
import functools

import jax
import jax.numpy as jnp
from jax import lax
from jax.experimental import pallas as pl
from jax.experimental.pallas import tpu as pltpu
from jax.sharding import PartitionSpec as P

DHK = 128
DHV = 256
EPS = 1e-06
ROWS = 16
MESH = pl.DeviceIdType.MESH
F32 = jnp.float32
BF16 = jnp.bfloat16


def kernel(T, N, *refs):
    (x_in, *rest) = refs
    ins = (rest[:11], rest[11:22])
    outs = rest[22:29]
    (
        wcat,
        wmix,
        wif,
        wif_own,
        gains,
        cell,
        norm,
        stab,
        cellt_hi,
        cellt_lo,
        xl,
        xg,
        xs,
        xres_send,
        xres,
        stage,
        sbuf,
        rbuf,
        gbuf,
        gs,
        ybuf,
        ysc,
        ysend,
        yrecv,
        load_sems,
        pair_send,
        pair_recv,
        send_sems,
        recv_sems,
    ) = rest[29:]
    t = lax.axis_index("tp")
    d = lax.axis_index("dp")
    Z = N // 2
    c = lax.rem(d, 2)
    z = d // 2
    partner = {"dp": 2 * z + 1 - c}
    features = DHK * N

    TX = 4 if T % 4 == 0 else T
    TY = T // TX
    plane = [(dy, dx) for dy in range(TY) for dx in range(TX)]
    plane.sort(key=lambda o: -(min(o[0], TY - o[0]) + min(o[1], TX - o[1])))
    far_z = sorted(range(1, Z), key=lambda o: abs(o - Z // 2))

    def tp_index(o):
        return lax.rem(t // TX + o[0], TY) * TX + lax.rem(lax.rem(t, TX) + o[1], TX)

    others = [tp_index(o) for o in plane[:-1]]

    def z_peer(o):
        return {"dp": 2 * lax.rem(z + o, Z) + c}

    barrier = pltpu.get_barrier_semaphore()

    def greet(peer):
        pl.semaphore_signal(barrier, inc=1, device_id=peer, device_id_type=MESH)

    for o in far_z:
        greet(z_peer(o))
    for j in others:
        for b in range(2):
            greet({"tp": j, "dp": 2 * z + b})
    greet(partner)

    x_loads = [
        pltpu.make_async_copy(x_in, xl, load_sems.at[0]),
        pltpu.make_async_copy(x_in.at[c], xg.at[2 * t + c], load_sems.at[1]),
    ]
    for copy in x_loads:
        copy.start()
    loads = []
    for n in range(2):
        gain, wq, wk, wv, wo, wi, wf, wm, state, nstate, mstate = ins[n]
        shared = [
            (gain, gains.at[n, c]),
            (wq, wcat.at[n, c, :, 0:128]),
            (wk, wcat.at[n, c, :, 128:256]),
            (wv, wcat.at[n, c, :, 256:512]),
            (wo, wcat.at[n, c, :, 512:768]),
            (wi, wif.at[n, c, 0]),
            (wf, wif.at[n, c, 1]),
            (wm, wmix.at[n, c]),
        ]
        private = [
            (state, cell.at[n]),
            (nstate, norm.at[n]),
            (mstate, stab.at[n]),
        ]
        group = []
        for i, (src, dst) in enumerate(shared + private):
            copy = pltpu.make_async_copy(src, dst, load_sems.at[2 + 11 * n + i])
            copy.start()
            group.append(copy)
        loads.append((shared, group))

    def prepare(n):
        for s in range(2):
            old = cell[n, s * DHV : (s + 1) * DHV, :]
            turned = old.T
            high = turned.astype(BF16)
            cellt_hi[n, :, s * DHV : (s + 1) * DHV] = high
            cellt_lo[n, :, s * DHV : (s + 1) * DHV] = (turned - high.astype(F32)).astype(BF16)

    def own_gates(n):
        mine = lax.broadcasted_iota(jnp.int32, (T, DHK), 0) == t
        for b in range(2):
            for g in range(2):
                wif_own[n, b, g] = jnp.sum(
                    jnp.where(mine, wif[n, b, g].astype(F32), 0.0), axis=0, keepdims=True
                )

    def send(src, dst, phase, peer):
        copy = pltpu.make_async_remote_copy(
            src_ref=src,
            dst_ref=dst,
            send_sem=send_sems.at[phase],
            recv_sem=recv_sems.at[phase],
            device_id=peer,
            device_id_type=MESH,
        )
        copy.start()

    def wait_recv(ref, phase):
        pltpu.make_async_copy(ref, ref, recv_sems.at[phase]).wait()

    def wait_send(ref, phase):
        pltpu.make_async_copy(ref, ref, send_sems.at[phase]).wait()

    sends = []
    pairs = []

    def share(n):
        for i, (src, dst) in enumerate(loads[n][0]):
            copy = pltpu.make_async_remote_copy(
                src_ref=src,
                dst_ref=dst,
                send_sem=pair_send.at[8 * n + i],
                recv_sem=pair_recv.at[8 * n + i],
                device_id=partner,
                device_id_type=MESH,
            )
            copy.start()
            pairs.append(copy)

    def ready(n):
        for copy in loads[n][1]:
            copy.wait()
        for copy in pairs[8 * n : 8 * n + 8]:
            copy.wait_recv()

    for copy in x_loads:
        copy.wait()
    with jax.named_scope("entry"):
        pl.semaphore_wait(barrier, Z - 1 + 2 * T - 1)

    for j in others:
        for b in range(2):
            send(xl.at[b], xg.at[2 * t + c], 0, {"tp": j, "dp": 2 * z + b})
    send(xl.at[1 - c], xg.at[2 * t + c], 0, partner)
    sends.append((xg.at[pl.ds(0, 2 * T - 1)], 0))
    share(0)
    with jax.named_scope("ready"):
        ready(0)
    own_gates(0)
    prepare(0)

    with jax.named_scope("x_wait"):
        wait_recv(xg.at[pl.ds(0, 2 * T - 1)], 0)
    for j in range(T):
        for b in range(2):
            xs[b, 2 * j : 2 * j + 2, :] = xg[2 * j + b].astype(F32)

    def project(n, phase):
        wide = [
            jnp.concatenate(
                [xs[b, pl.ds(0, Z, stride=2), :], xs[b, pl.ds(1, Z, stride=2), :]], axis=0
            )
            for b in range(2)
        ]
        scaled = [(wide[b] * gains[n, b].astype(F32)).astype(BF16) for b in range(2)]
        product = jnp.dot(scaled[0], wcat[n, 0], preferred_element_type=F32) + jnp.dot(
            scaled[1], wcat[n, 1], preferred_element_type=F32
        )
        squares = jnp.sum(wide[0] * wide[0] + wide[1] * wide[1], axis=1, keepdims=True)
        again = [scaled[b].astype(F32) for b in range(2)]
        gate_parts = [
            jnp.sum(
                again[0] * wif_own[n, 0, g] + again[1] * wif_own[n, 1, g], axis=1, keepdims=True
            )
            for g in range(2)
        ]
        lane = lax.broadcasted_iota(jnp.int32, (2 * Z, 128), 1)
        misc = jnp.where(lane == 0, gate_parts[0], jnp.where(lane == 1, gate_parts[1], squares))
        high = misc.astype(BF16).astype(F32)
        low = misc - high
        blocks = [product[:, 128 * b : 128 * (b + 1)] for b in range(6)] + [high, low]
        for b, block in enumerate(blocks):
            for s in range(2):
                stage[pl.ds(2 * b + s, Z, stride=ROWS), :] = block[s * Z : (s + 1) * Z]
        sbuf[n] = stage[...].reshape(Z, ROWS, 128).astype(BF16)
        for o in far_z:
            send(sbuf.at[n, lax.rem(z + o, Z)], rbuf.at[n, Z - 1 - o], phase, z_peer(o))
        sends.append((rbuf.at[n], phase))

    def step_state(n, phase_in, phase_out):
        with jax.named_scope("rs_wait"):
            wait_recv(rbuf.at[n], phase_in)
        acc = sbuf[n, z].astype(F32) + jnp.sum(rbuf[n].astype(F32), axis=0)
        acc_hi = acc.astype(BF16)
        acc_lo = (acc - acc_hi.astype(F32)).astype(BF16)
        read = (
            jnp.dot(acc_hi, cellt_hi[n], preferred_element_type=F32)
            + jnp.dot(acc_lo, cellt_hi[n], preferred_element_type=F32)
            + jnp.dot(acc_hi, cellt_lo[n], preferred_element_type=F32)
        )
        row = lax.broadcasted_iota(jnp.int32, (2, DHV), 0)
        read = jnp.where(row == 0, read[0:2, 0:DHV], read[0:2, DHV : 2 * DHV])
        q0 = acc[0:2]
        k0 = acc[2:4]
        v0 = jnp.concatenate([acc[4:6], acc[6:8]], axis=1)
        o0 = jnp.concatenate([acc[8:10], acc[10:12]], axis=1)
        misc = acc[12:14] + acc[14:16]
        lane = lax.broadcasted_iota(jnp.int32, (2, 128), 1)
        i0 = jnp.sum(jnp.where(lane == 0, misc, 0.0), axis=1, keepdims=True)
        f0 = jnp.sum(jnp.where(lane == 1, misc, 0.0), axis=1, keepdims=True)
        squares = jnp.sum(jnp.where(lane == 2, misc, 0.0), axis=1, keepdims=True)
        kq0 = jnp.sum(k0 * q0, axis=1, keepdims=True)
        nq0 = jnp.sum(norm[n] * q0, axis=1, keepdims=True)
        r = lax.rsqrt(squares / features + EPS)
        rq = r * DHK ** (-0.5)
        i_pre = i0 * r
        f_pre = f0 * r
        pick = lax.broadcasted_iota(jnp.int32, (2, 2), 0) == lax.broadcasted_iota(jnp.int32, (2, 2), 1)
        m = jnp.sum(jnp.where(pick, stab[n], 0.0), axis=1, keepdims=True)
        lf = jnp.minimum(f_pre, 0.0) - jnp.log1p(jnp.exp(-jnp.abs(f_pre)))
        m_next = jnp.maximum(lf + m, i_pre)
        retain = jnp.exp(lf + m - m_next)
        admit = jnp.exp(i_pre - m_next)
        kq = kq0 * r * rq
        den = retain * (nq0 * rq) + admit * kq
        num = (retain * rq) * read + (admit * kq) * (v0 * r)
        gated = num / jnp.maximum(jnp.abs(den), 1.0) * jax.nn.sigmoid(o0 * r)
        gbuf[n, z] = gated.astype(BF16)
        for o in far_z:
            send(gbuf.at[n, z], gbuf.at[n, z], phase_out, z_peer(o))
        sends.append((gbuf.at[n, pl.ds(0, Z - 1)], phase_out))
        c_out, n_out, m_out = outs[1 + 3 * n : 4 + 3 * n]
        k = k0 * r
        n_out[...] = retain * norm[n] + admit * k
        m_out[...] = jnp.sum(jnp.where(pick, m_next, 0.0), axis=0, keepdims=True)
        va = v0 * (r * admit)
        for s in range(2):
            column = jnp.broadcast_to(va[s : s + 1], (8, DHV)).T[:, 0:1]
            c_out[s * DHV : (s + 1) * DHV, :] = (
                retain[s : s + 1] * cell[n, s * DHV : (s + 1) * DHV, :] + column * k[s : s + 1]
            )

    def mix(n, phase_in):
        with jax.named_scope("ag_wait"):
            wait_recv(gbuf.at[n, pl.ds(0, Z - 1)], phase_in)
        for j in range(Z):
            gs[2 * j : 2 * j + 2, :] = gbuf[n, j].astype(F32)
        rows = gs[...].astype(BF16)
        return [jnp.dot(rows, wmix[n, b], preferred_element_type=F32) for b in range(2)]

    project(0, 1)
    share(1)
    with jax.named_scope("ready"):
        ready(1)
    own_gates(1)
    prepare(1)
    step_state(0, 1, 2)
    partial = mix(0, 2)
    for b in range(2):
        ybuf[t, b] = partial[b].astype(BF16)
    for j in others:
        send(ybuf.at[t], ybuf.at[t], 3, {"tp": j})
    sends.append((ybuf.at[pl.ds(0, T - 1)], 3))
    with jax.named_scope("ar_wait"):
        wait_recv(ybuf.at[pl.ds(0, T - 1)], 3)
    for b in range(2):
        middle = xs[b] + jnp.sum(ybuf[:, b].astype(F32), axis=0)
        xs[b] = middle.astype(BF16).astype(F32)
    project(1, 4)
    xres_send[...] = xs[1 - c, pl.ds(2 * t, 2), :].astype(BF16)
    send(xres_send, xres, 6, partner)
    sends.append((xres_send, 6))
    step_state(1, 4, 5)
    last = mix(1, 5)
    for b in range(2):
        ysc[b] = last[b]
    for j in range(T):
        for b in range(2):
            ysend[2 * j + b] = ysc[b, 2 * j : 2 * j + 2, :].astype(BF16)
    for j in others:
        for b in range(2):
            send(ysend.at[2 * j + b], yrecv.at[c * T + t], 7, {"tp": j, "dp": 2 * z + b})
    send(ysend.at[2 * t + 1 - c], yrecv.at[c * T + t], 7, partner)
    sends.append((yrecv.at[pl.ds(0, 2 * T - 1)], 7))
    yrecv[c * T + t] = ysend[2 * t + c]
    wait_recv(xres, 6)
    with jax.named_scope("y_wait"):
        wait_recv(yrecv.at[pl.ds(0, 2 * T - 1)], 7)
    own_x = xs[c, pl.ds(2 * t, 2), :]
    other_x = xres[...].astype(F32)
    for b in range(2):
        stream = jnp.where(c == b, own_x, other_x)
        total = jnp.sum(yrecv[b * T : (b + 1) * T].astype(F32), axis=0)
        outs[0][b] = (stream + total).astype(BF16)
    for ref, phase in sends:
        wait_send(ref, phase)
    for copy in pairs:
        copy.wait_send()


def publish(*refs):
    sems = refs[14]
    copies = [pltpu.make_async_copy(refs[n], refs[7 + n], sems.at[n]) for n in range(7)]
    for copy in copies:
        copy.start()
    for copy in copies:
        copy.wait()


def build(T, N):
    def per_device(*args):
        flat = [args[0].reshape(2, 2, DHK)]
        for n in range(2):
            gain, wq, wk, wv, wo, wi, wf, wm, state, nstate, mstate = args[1 + 11 * n : 12 + 11 * n]
            flat += [
                gain.reshape(1, DHK),
                wq,
                wk,
                wv,
                wo,
                wi.T,
                wf.T,
                wm,
                state.reshape(2 * DHV, DHK),
                nstate.reshape(2, DHK),
                mstate.T,
            ]
        hbm = pl.BlockSpec(memory_space=pltpu.HBM)
        vmem = pl.BlockSpec(memory_space=pltpu.VMEM)
        state_shapes = [
            ((2 * DHV, DHK), F32),
            ((2, DHK), F32),
            ((1, 2), F32),
        ]
        shapes = [((2, 2, DHK), BF16)] + state_shapes * 2
        Z = N // 2
        half = 2 * Z
        got = pl.pallas_call(
            functools.partial(kernel, T, N),
            out_shape=[pltpu.VMEM(*shape) for shape in shapes],
            in_specs=[hbm] * len(flat),
            out_specs=[vmem] * 7,
            scratch_shapes=[
                pltpu.VMEM((2, 2, DHK, 768), BF16),
                pltpu.VMEM((2, 2, DHV, DHK), BF16),
                pltpu.VMEM((2, 2, 2, T, DHK), BF16),
                pltpu.VMEM((2, 2, 2, 1, DHK), F32),
                pltpu.VMEM((2, 2, 1, DHK), BF16),
                pltpu.VMEM((2, 2 * DHV, DHK), F32),
                pltpu.VMEM((2, 2, DHK), F32),
                pltpu.VMEM((2, 1, 2), F32),
                pltpu.VMEM((2, DHK, 2 * DHV), BF16),
                pltpu.VMEM((2, DHK, 2 * DHV), BF16),
                pltpu.VMEM((2, 2, DHK), BF16),
                pltpu.VMEM((2 * T, 2, DHK), BF16),
                pltpu.VMEM((2, half, DHK), F32),
                pltpu.VMEM((2, DHK), BF16),
                pltpu.VMEM((2, DHK), BF16),
                pltpu.VMEM((Z * ROWS, DHK), F32),
                pltpu.VMEM((2, Z, ROWS, DHK), BF16),
                pltpu.VMEM((2, Z - 1, ROWS, DHK), BF16),
                pltpu.VMEM((2, Z, 2, DHV), BF16),
                pltpu.VMEM((half, DHV), F32),
                pltpu.VMEM((T, 2, half, DHK), BF16),
                pltpu.VMEM((2, half, DHK), F32),
                pltpu.VMEM((2 * T, 2, DHK), BF16),
                pltpu.VMEM((2 * T, 2, DHK), BF16),
                pltpu.SemaphoreType.DMA((24,)),
                pltpu.SemaphoreType.DMA((16,)),
                pltpu.SemaphoreType.DMA((16,)),
                pltpu.SemaphoreType.DMA((8,)),
                pltpu.SemaphoreType.DMA((8,)),
            ],
            compiler_params=pltpu.CompilerParams(
                collective_id=0, has_side_effects=True, vmem_limit_bytes=24 * 1024 * 1024
            ),
            name="cells",
        )(*[pltpu.with_memory_space_constraint(a, pltpu.HBM) for a in flat])
        got = pl.pallas_call(
            publish,
            out_shape=[jax.ShapeDtypeStruct(*shape) for shape in shapes],
            in_specs=[vmem] * 7,
            out_specs=[hbm] * 7,
            scratch_shapes=[pltpu.SemaphoreType.DMA((7,))],
            compiler_params=pltpu.CompilerParams(vmem_limit_bytes=1024 * 1024),
            name="publish",
        )(*got)
        hidden, c1, n1, m1, c2, n2, m2 = got
        return (
            hidden.reshape(4, DHK),
            c1.reshape(2, 1, DHV, DHK),
            n1.reshape(2, 1, DHK),
            m1.T,
            c2.reshape(2, 1, DHV, DHK),
            n2.reshape(2, 1, DHK),
            m2.T,
        )

    return per_device


def solution(mesh):
    cell_specs = (
        P("dp"),
        P("dp", "tp"),
        P("dp", "tp"),
        P("dp", "tp"),
        P("dp", "tp"),
        P("dp", None),
        P("dp", None),
        P("tp", "dp"),
        P("dp", "tp", None, None),
        P("dp", "tp", None),
        P("dp", "tp"),
    )
    state_specs = (P("dp", "tp", None, None), P("dp", "tp", None), P("dp", "tp"))
    return jax.shard_map(
        build(mesh.shape["tp"], mesh.shape["dp"]),
        mesh=mesh,
        in_specs=(P("tp", "dp"),) + cell_specs * 2,
        out_specs=(P("tp", "dp"),) + state_specs * 2,
        check_vma=False,
    )
```

time: 67 us -> 64.2 us (0.958)
  Pallas kernels: 66.2 us -> 63.5 us
    pallas_call x1, Pallas kernels: 65.3 us -> 62.6 us  [per_device(): pl.pallas_call(functools.partial(kernel, T, N), out_shape=[pltpu.VMEM(*sh...]
where the time goes in v3:
time: 64.2 us; the launch traced here: 64.1 us
  Pallas kernels  63.5 us (99%)
  between operations  0.65 us (1%)
    pallas_call x1, Pallas kernels, per_device(): pl.pallas_call(functools.partial(kernel, T, N), out_shape=[pltpu.VMEM(*sh...  62.6 us

profile of v3, /device:TPU:1, one launch (start us, length us, event | category | flops | bytes accessed | tf_op | source)
XLA Modules:
  0.0 64.1 jit_solution(16370547811589059932)
XLA Ops:
  0.6 62.6 %cells.1 = (bf16[2,2,128]{2,1,0:T(2,128)(2,1)S(1)}, f32[512,128]{1,0:T(8,128)S(1)}, f32[2,128]{1,0:T(2,128)S(1)}, f32[1,2]{1,0:T(1,128)S(1)}, f32[512,128]{1,0:T...) custom-call(bf16[2,2,128]{2,1,0:T(2,128)(2,1)} %bitcast.34, bf16[1,128]{1,0:T(2,128)(2,1)} %bitcast.37, ...), custom_call_target="tpu_custom_call" | custom-call | tf_op jit(solution)/shard_map/cells/pallas_call | solution.py:376
  63.2 0.9 %publish.1 = (bf16[2,2,128]{2,1,0:T(2,128)(2,1)}, f32[512,128]{1,0:T(8,128)}, f32[2,128]{1,0:T(2,128)}, f32[1,2]{1,0:T(1,128)}, f32[512,128]{1,0:T(8,128)}, /*index=5*/f32[2,128]{1,0:T(2,128)}, f32[1,2]{1,0:T(1,128)}) custom-call(bf16[2,2,128]{2,1,0:T(2,128)(2,1)S(1)} %get-tuple-element.21.refs_0_, f32[512,128]{1,0:T(8,128)S(1)} %get-tuple-element.22.refs_1_, ...), custom_call_target="tpu_custom_call" | custom-call | tf_op jit(solution)/shard_map/publish/pallas_call | solution.py:417
